TPU v7x, 128 devices: a whole 4x4x4 slice. The times are simulated.
128 devices in a mesh: rep: 2 (over z_hi), fs: 32 (over z_lo, y, x), tp: 2 (over core).
Axes of the slice: x: 4, y: 4, z: 4 (z_hi: 2, z_lo: 2; z = z_hi * 2 + z_lo), core: 2. Of those that a mesh axis runs over, the one named last changes fastest.
Arguments:
- tokens: bfloat16 [40960, 2048], P(('rep', 'fs'), 'tp'), may hold values from -6 to 6
- norm_first: float32 [2048], replicated, may hold values from 0.1 to 1.9
- norm_mix: float32 [2048], replicated, may hold values from 0.1 to 1.9
- norm_second: float32 [2048], replicated, may hold values from 0.1 to 1.9
- gate_weight: float32 [2048, 2816], P('fs', 'tp'), may hold values from -0.125 to 0.125
- up_weight: float32 [2048, 2816], P('fs', 'tp'), may hold values from -0.125 to 0.125
- down_weight: float32 [2816, 2048], P('tp', 'fs'), may hold values from -0.109375 to 0.109375
- gate_scale: float32 [2816], P('tp'), may hold values from 0.3 to 3
- up_scale: float32 [2816], P('tp'), may hold values from 0.3 to 3
- down_scale: float32 [2048], P('fs'), may hold values from 0.3 to 3
- u_weight: float32 [2048, 1024], P('fs', 'tp'), may hold values from -0.125 to 0.125
- v_weight: float32 [2048, 1024], P('fs', 'tp'), may hold values from -0.125 to 0.125
- u_scale: float32 [1024], P('tp'), may hold values from 0.3 to 3
- v_scale: float32 [1024], P('tp'), may hold values from 0.15 to 6
- ln_gain: float32 [1024], P('tp'), may hold values from 0.1 to 1.9
- ln_bias: float32 [1024], P('tp'), may hold values from -3 to 3
- spatial_weight: bfloat16 [8, 128, 128], P('tp'), may hold values from -0.25 to 0.25
- spatial_bias: float32 [8, 128], P('tp'), may hold values from 0.1 to 1.9
- out_weight: float32 [1024, 2048], P('tp', 'fs'), may hold values from -0.1875 to 0.1875
- out_scale: float32 [2048], P('fs'), may hold values from 0.3 to 3
Outputs:
- layer_out: bfloat16 [40960, 2048], P(('rep', 'fs'), 'tp')
All inputs are finite; a program needn't handle non-finite values.
Results may differ from a plain program's by a relative error of at most 0.019.
Values may be sent and summed in bfloat16 or wider, within the bound.
A program may use at most 128 MiB of HBM per device.

v0:
```python
import jax
import jax.numpy as jnp
from jax import lax
from jax.sharding import Mesh
from jax.sharding import PartitionSpec as P

BW = 1024
SPAN = 128
FS = ("fs_0", "fs_1", "fs_2")
REP_FS = ("rep", "fs_0", "fs_1", "fs_2")


EPS = 1e-06


def rows_first(arrays, axis, dims):
    turned = [jnp.moveaxis(a, dim, 0) for a, dim in zip(arrays, dims)]
    both = jnp.concatenate([t.reshape(len(t), -1) for t in turned], axis=1)
    result, at, done = (lax.all_gather(both, axis, axis=0, tiled=True), 0, [])
    for t, dim in zip(turned, dims):
        slab = result[:, at : at + t[0].size].reshape(-1, *t.shape[1:])
        done.append(jnp.moveaxis(slab, 0, dim))
        at += t[0].size
    return tuple(done)


def sent_to_all(x, axis):
    size = lax.axis_size(axis)
    return lax.all_to_all(jnp.broadcast_to(x[None], (size, *x.shape)), axis, 0, 0, tiled=True)


def in_order(parts, dim):
    dims = list(parts.shape[1:])
    dims[dim] *= parts.shape[0]
    return jnp.moveaxis(parts, 0, dim).reshape(dims)


def gather_directly(x, axis, dim):
    parts = sent_to_all(x, axis)
    return in_order(parts, dim)


def cut_along(x, dim, size):
    dims = x.shape
    parts = x.reshape(*dims[:dim], size, dims[dim] // size, *dims[dim + 1 :])
    return jnp.moveaxis(parts, dim, 0)


def sum_at_owner(x, axis, dim):
    parts = cut_along(x, dim, lax.axis_size(axis))
    arrived = lax.all_to_all(parts, axis, split_axis=0, concat_axis=0, tiled=True)
    return arrived.astype(jnp.float32).sum(axis=0)


def sent_together(arrays, axis, dim, along):
    ends, at = ([], 0)
    for a in arrays[:-1]:
        at += a.shape[along]
        ends.append(at)
    both = jnp.concatenate(arrays, axis=along)
    return tuple(jnp.split(lax.all_gather(both, axis, axis=dim, tiled=True), ends, axis=along))


def gather_in_order(x, axes, turns):
    parts = x
    for k in turns:
        parts = lax.all_gather(parts, axes[k])
    done = turns[::-1]
    back = [done.index(k) for k in range(len(axes))]
    parts = parts.transpose(*back, *range(len(axes), parts.ndim))
    return parts.reshape(-1, *x.shape)


def whole_of(x, axes, turns, dim):
    return in_order(gather_in_order(x, axes, turns), dim)


def of_everyone(x, axis):
    return sent_to_all(x, axis).sum(axis=0)


def together(arrays, axis):
    ends = [0]
    for a in arrays:
        ends.append(ends[-1] + a.size)
    so_far = of_everyone(jnp.concatenate([a.ravel() for a in arrays]), axis)
    return tuple((so_far[b:e].reshape(a.shape) for a, b, e in zip(arrays, ends, ends[1:])))


def add_pair(left, pieces):
    return (
        jnp.dot(left, pieces[0], preferred_element_type=jnp.float32),
        jnp.dot(left, pieces[1], preferred_element_type=jnp.float32),
    )


def on_device(
    tokens,
    norm_first,
    norm_mix,
    norm_second,
    gate_weight,
    up_weight,
    down_weight,
    gate_scale,
    up_scale,
    down_scale,
    u_weight,
    v_weight,
    u_scale,
    v_scale,
    ln_gain,
    ln_bias,
    spatial_weight,
    spatial_bias,
    out_weight,
    out_scale,
):
    wide_scales = rows_first((down_scale, out_scale), FS, (0, 0))
    gate_low = gate_weight.astype(jnp.bfloat16)
    up_low = up_weight.astype(jnp.bfloat16)
    down_low = down_weight.astype(jnp.bfloat16)
    count = tokens.shape[0]

    def full_norm(rows, gain):
        whole = gather_directly(rows, "tp", 1)
        values = whole.astype(jnp.float32)
        factor = lax.rsqrt(jnp.mean(values * values, axis=1, keepdims=True) + EPS)
        return (values * factor * gain).astype(jnp.bfloat16)

    def spread_sum(term):
        return sum_at_owner(term.astype(jnp.bfloat16), "tp", 1)

    gate_all, up_all = sent_together((gate_low, up_low), FS, 0, 1)

    def hidden_units(normed):
        gate = jnp.dot(normed, gate_all, preferred_element_type=jnp.float32) * gate_scale
        up_part = jnp.dot(normed, up_all, preferred_element_type=jnp.float32) * up_scale
        return (jax.nn.silu(gate) * up_part).astype(jnp.bfloat16)

    first_hidden = hidden_units(full_norm(tokens, norm_first))
    down_all = whole_of(down_low, FS, (0, 1, 2), 1)
    first_term = (
        jnp.dot(first_hidden, down_all, preferred_element_type=jnp.float32) * wide_scales[0]
    )
    first = spread_sum(first_term)
    middle = (tokens.astype(jnp.float32) + 0.5 * first).astype(jnp.bfloat16)
    mix_normed = full_norm(middle, norm_mix)
    u_low = u_weight.astype(jnp.bfloat16)
    v_low = v_weight.astype(jnp.bfloat16)
    u_acc, v_acc = add_pair(mix_normed, sent_together((u_low, v_low), FS, 0, 1))
    u_pre = u_acc * u_scale
    v_act = jax.nn.gelu(v_acc * v_scale, approximate=True)
    totals = together((jnp.sum(v_act, axis=1), jnp.sum(v_act * v_act, axis=1)), "tp")
    v_mean = (totals[0] / BW)[:, None]
    v_var = (totals[1] / BW)[:, None] - v_mean * v_mean
    v_normed = ((v_act - v_mean) * lax.rsqrt(v_var + EPS) * ln_gain + ln_bias).astype(jnp.bfloat16)
    local_groups = spatial_weight.shape[0]
    channels = v_act.shape[1] // local_groups
    blocks = v_normed.reshape(count // SPAN, SPAN, local_groups, channels)
    lower = jnp.tril(jnp.ones((SPAN, SPAN), jnp.bool_))
    masked = jnp.where(lower[None], spatial_weight, jnp.zeros_like(spatial_weight))
    spatial = jnp.einsum("gts,nsgc->ntgc", masked, blocks, preferred_element_type=jnp.float32)
    spatial = spatial + spatial_bias.T[None, :, :, None]
    mixed = (jax.nn.gelu(u_pre, approximate=True) * spatial.reshape(count, v_act.shape[1])).astype(
        jnp.bfloat16
    )
    out_low = out_weight.astype(jnp.bfloat16)
    mix_term = (
        jnp.dot(mixed, gather_directly(out_low, FS, 1), preferred_element_type=jnp.float32)
        * wide_scales[1]
    )
    second = (middle.astype(jnp.float32) + spread_sum(mix_term)).astype(jnp.bfloat16)
    second_hidden = hidden_units(full_norm(second, norm_second))
    last = spread_sum(
        jnp.dot(second_hidden, down_all, preferred_element_type=jnp.float32) * wide_scales[0]
    )
    return (second.astype(jnp.float32) + 0.5 * last).astype(jnp.bfloat16)


def solution(mesh):
    torus = Mesh(
        mesh.devices.reshape(mesh.shape["rep"], 2, 4, 4, mesh.shape["tp"]),
        ("rep", "fs_0", "fs_1", "fs_2", "tp"),
    )
    in_specs = (
        P(REP_FS, "tp"),
        P(),
        P(),
        P(),
        P(FS, "tp"),
        P(FS, "tp"),
        P("tp", FS),
        P("tp"),
        P("tp"),
        P(FS),
        P(FS, "tp"),
        P(FS, "tp"),
        P("tp"),
        P("tp"),
        P("tp"),
        P("tp"),
        P("tp", None, None),
        P("tp", None),
        P("tp", FS),
        P(FS),
    )
    out_specs = P(REP_FS, "tp")
    return jax.shard_map(
        on_device, mesh=torus, in_specs=in_specs, out_specs=out_specs, check_vma=False
    )
```

profile of v0, /device:TPU:1, one launch (start us, length us, event | category | flops | bytes accessed | tf_op | source)
XLA Modules:
  0.0 554.3 jit_solution(2388582558975060697)
XLA Ops:
  7.6 7.5 %all-gather = bf16[2816,64]{0,1:T(8,128)(2,1)S(1)} all-gather(bf16[1408,64]{0,1:T(8,128)(2,1)S(1)} %convert_element_type.123), channel_id=2, replica_groups=mesh['rep'=2,'fs_0'=2,'fs_1'=4,'fs_2'=4,'tp'=2] {'fs_0'}, dimensions={0}, use_global_device_ids=true | all-gather | bytes 540672 | tf_op jit(solution)/shard_map/all_gather | solution.py:67
  16.0 28.1 %all-gather.13.cloned.1.call-done = bf16[8,1408,64]{1,2,0:T(8,128)(2,1)} async-done(((bf16[2,1408,64]{1,2,0:T(8,128)(2,1)}), bf16[8,1408,64]{1,2,0:T(8,128)(2,1)}) %all-gather.13.cloned.1.call-update) | async-done | bytes 1441808 | tf_op jit(solution)/shard_map/all_gather | solution.py:67
  48.4 4.8 all-to-all-start
  53.2 68.0 %all-gather.3 = f32[32,64,2]{1,2,0:T(2,128)S(1)} all-gather(f32[1,64,2]{1,2,0:T(2,128)S(1)} %maximum_bitcast_fusion), channel_id=1, replica_groups=mesh['rep'=2,'fs_0'=2,'fs_1'=4,'fs_2'=4,'tp'=2] {'fs_0','fs_1','fs_2'}, dimensions={0}, use_global_device_ids=true | all-gather | bytes 16896 | tf_op jit(solution)/shard_map/all_gather | solution.py:19
  121.9 2.2 fusion.5
  124.2 5.8 %copy.78 = bf16[2,4,4,1408,64]{3,4,2,1,0:T(8,128)(2,1)} copy(bf16[2,4,4,1408,64]{3,4,0,1,2:T(8,128)(2,1)} %bitcast.99) | data formatting | bytes 11534336 | tf_op jit(solution)/shard_map/transpose | solution.py:70
  130.0 132.8 %all-gather.9.cloned.1.call-done = bf16[2048,2816]{1,0:T(8,128)(2,1)} async-done(((bf16[64,2816]{1,0:T(8,128)(2,1)}), bf16[2048,2816]{1,0:T(8,128)(2,1)}) %all-gather.9.cloned.1.call-update) | async-done | bytes 11534352 | tf_op jit(solution)/shard_map/all_gather | solution.py:61
  262.8 8.7 %fusion.14 = f32[640,1408]{1,0:T(8,128)} fusion(bf16[640,2048]{0,1:T(8,128)(2,1)S(1)} %copy-done.2, bf16[2048,2816]{1,0:T(8,128)(2,1)} %all-gather.9.cloned.1.call-done, f32[1408]{0:T(1024)S(1)} %copy-done.18), kind=kOutput, calls=%fused_computation.26 | convolution fusion | flops 3691888640 | bytes 11998720 | tf_op jit(solution)/shard_map/dot_general | solution.py:137
  271.5 14.9 %multiply_convert_fusion.2 = bf16[640,2048]{1,0:T(8,128)(2,1)S(1)} fusion(bf16[1408,2048]{0,1:T(8,128)(2,1)} %bitcast.97, f32[2048]{0:T(1024)S(1)} %bitcast.107, bf16[640,2048]{0,1:T(8,128)(2,1)} %fusion.5, bf16[2048,2816]{1,0:T(8,128)(2,1)} %all-gather.9.cloned.1.call-done, f32[640,1408]{1,0:T(8,128)} %fusion.14, f32[1408]{0:T(1024)S(1)} %copy-done.19), kind=kOutput, calls=%fused_computation.16 | convolution fusion | flops 7390904320 | bytes 20395520 | tf_op jit(solution)/shard_map/dot_general | solution.py:144
  286.6 25.1 %all_to_all.41 = bf16[2,640,1024]{2,1,0:T(8,128)(2,1)S(1)} all-to-all(bf16[2,640,1024]{2,1,0:T(8,128)(2,1)S(1)} %bitcast.94), channel_id=1, replica_groups=mesh['rep'=2,'fs_0'=2,'fs_1'=4,'fs_2'=4,'tp'=2] {'tp'}, dimensions={0} | all-to-all | bytes 5242880 | tf_op jit(solution)/shard_map/all_to_all | solution.py:51
  314.5 5.8 %all_to_all.42 = bf16[2,640,1024]{1,2,0:T(8,128)(2,1)S(1)} all-to-all(bf16[2,640,1024]{1,2,0:T(8,128)(2,1)S(1)} %broadcast_in_dim.19), channel_id=1, replica_groups=mesh['rep'=2,'fs_0'=2,'fs_1'=4,'fs_2'=4,'tp'=2] {'tp'}, dimensions={0} | all-to-all | bytes 5242880 | tf_op jit(solution)/shard_map/all_to_all | solution.py:29
  321.0 2.2 fusion.3
  323.2 95.5 %all-gather.11.cloned.1.call-done = bf16[2048,1024]{1,0:T(8,128)(2,1)} async-done(((bf16[64,1024]{1,0:T(8,128)(2,1)}), bf16[2048,1024]{1,0:T(8,128)(2,1)}) %all-gather.11.cloned.1.call-update) | async-done | bytes 4194320 | tf_op jit(solution)/shard_map/all_gather | solution.py:61
  418.7 5.4 fusion.90
  424.0 24.0 %all_to_all.43 = f32[2,1,1280]{2,1,0:T(1,128)S(1)} all-to-all(f32[2,1,1280]{2,1,0:T(1,128)S(1)} %broadcast_in_dim.20), channel_id=1, replica_groups=mesh['rep'=2,'fs_0'=2,'fs_1'=4,'fs_2'=4,'tp'=2] {'tp'}, dimensions={0} | all-to-all | bytes 20480 | tf_op jit(solution)/shard_map/all_to_all | solution.py:29
  449.6 7.2 %all-to-all-start.4 = ((bf16[32,512,64]{1,2,0:T(8,128)(2,1)}), bf16[32,512,64]{1,2,0:T(8,128)(2,1)}, u32[]{:S(2)}, u32[]{:S(2)}) async-start(bf16[32,512,64]{1,2,0:T(8,128)(2,1)} %broadcast_in_dim.23), calls=%async_computation.4 | async-start | bytes 4194304 | tf_op jit(solution)/shard_map/all_to_all | solution.py:29
  460.6 23.1 %all-to-all-done.4 = bf16[32,512,64]{1,2,0:T(8,128)(2,1)} async-done(((bf16[32,512,64]{1,2,0:T(8,128)(2,1)}), bf16[32,512,64]{1,2,0:T(8,128)(2,1)}, u32[]{:S(2)}, u32[]{:S(2)}) %all-to-all-start.4) | async-done | bytes 2097184 | tf_op jit(solution)/shard_map/all_to_all | solution.py:29
  483.7 8.1 %multiply_convert_fusion.1 = bf16[640,2048]{1,0:T(8,128)(2,1)} fusion(bf16[512,2048]{0,1:T(8,128)(2,1)} %bitcast.20, f32[2048]{0:T(1024)S(1)} %bitcast.109, f32[80,8,4,128]{3,2,1,0:T(4,128)} %bitcast.106, bf16[640,2048]{0,1:T(8,128)(2,1)} %fusion.3, bf16[2048,1024]{1,0:T(8,128)(2,1)} %all-gather.11.cloned.1.call-done, f32[512]{0:T(512)S(1)} %copy-done.21), kind=kOutput, calls=%fused_computation.13 | convolution fusion | flops 2690580480 | bytes 10758144 | tf_op jit(solution)/shard_map/dot_general | solution.py:170
  491.9 2.0 copy.109
  493.9 7.6 %all_to_all.44 = bf16[2,640,1024]{2,1,0:T(8,128)(2,1)S(1)} all-to-all(bf16[2,640,1024]{2,1,0:T(8,128)(2,1)S(1)} %bitcast.95), channel_id=1, replica_groups=mesh['rep'=2,'fs_0'=2,'fs_1'=4,'fs_2'=4,'tp'=2] {'tp'}, dimensions={0} | all-to-all | bytes 5242880 | tf_op jit(solution)/shard_map/all_to_all | solution.py:51
  503.5 6.0 %all_to_all.45 = bf16[2,640,1024]{1,2,0:T(8,128)(2,1)S(1)} all-to-all(bf16[2,640,1024]{1,2,0:T(8,128)(2,1)S(1)} %broadcast_in_dim.24), channel_id=1, replica_groups=mesh['rep'=2,'fs_0'=2,'fs_1'=4,'fs_2'=4,'tp'=2] {'tp'}, dimensions={0} | all-to-all | bytes 5242880 | tf_op jit(solution)/shard_map/all_to_all | solution.py:29
  512.4 8.7 %fusion.17 = f32[640,1408]{1,0:T(8,128)} fusion(bf16[640,2048]{0,1:T(8,128)(2,1)S(1)} %fusion.1, bf16[2048,2816]{1,0:T(8,128)(2,1)} %all-gather.9.cloned.1.call-done, f32[1408]{0:T(1024)S(1)} %copy-done.18), kind=kOutput, calls=%fused_computation.27 | convolution fusion | flops 3691888640 | bytes 11998720 | tf_op jit(solution)/shard_map/dot_general | solution.py:137
  521.1 16.5 %multiply_convert_fusion = bf16[640,2048]{1,0:T(8,128)(2,1)} fusion(bf16[1408,2048]{0,1:T(8,128)(2,1)} %bitcast.98, f32[2048]{0:T(1024)S(1)} %bitcast.108, bf16[640,2048]{0,1:T(8,128)(2,1)} %copy-done.3, bf16[2048,2816]{1,0:T(8,128)(2,1)} %all-gather.9.cloned.1.call-done, f32[640,1408]{1,0:T(8,128)} %fusion.17, f32[1408]{0:T(1024)S(1)} %copy-done.19), kind=kOutput, calls=%fused_computation.10 | convolution fusion | flops 7390904320 | bytes 20395520 | tf_op jit(solution)/shard_map/dot_general | solution.py:176
  539.5 5.8 %all_to_all.46 = bf16[2,640,1024]{2,1,0:T(8,128)(2,1)S(1)} all-to-all(bf16[2,640,1024]{2,1,0:T(8,128)(2,1)S(1)} %bitcast.96), channel_id=1, replica_groups=mesh['rep'=2,'fs_0'=2,'fs_1'=4,'fs_2'=4,'tp'=2] {'tp'}, dimensions={0} | all-to-all | bytes 5242880 | tf_op jit(solution)/shard_map/all_to_all | solution.py:51
  (98 shorter events, 24.8 us)
Async XLA Ops:
  6.5 37.6 %copy-start.4 = (f32[64,1408]{1,0:T(8,128)S(1)}, f32[64,1408]{1,0:T(8,128)}, u32[]{:S(2)}) copy-start(f32[64,1408]{1,0:T(8,128)} %param.24) | copy-start | bytes 1081348
  6.5 37.7 %copy-start.5 = (f32[64,1408]{1,0:T(8,128)S(1)}, f32[64,1408]{1,0:T(8,128)}, u32[]{:S(2)}) copy-start(f32[64,1408]{1,0:T(8,128)} %param.25) | copy-start | bytes 1081348
  6.5 37.6 %all-gather.13.cloned.1.call-start = ((), (), s32[]{:S(2)}) async-start(), calls=%async_computation.10 | async-start | bytes 1802240 | tf_op jit(solution)/shard_map/all_gather | solution.py:67
  7.6 37.5 %copy-start.7 = (f32[64,512]{1,0:T(8,128)S(1)}, f32[64,512]{1,0:T(8,128)}, u32[]{:S(2)}) copy-start(f32[64,512]{1,0:T(8,128)} %param.30) | copy-start | bytes 393220
  7.6 37.5 %copy-start.8 = (f32[64,512]{1,0:T(8,128)S(1)}, f32[64,512]{1,0:T(8,128)}, u32[]{:S(2)}) copy-start(f32[64,512]{1,0:T(8,128)} %param.31) | copy-start | bytes 393220
  15.1 30.7 %copy-start = (bf16[640,1024]{1,0:T(8,128)(2,1)S(1)}, bf16[640,1024]{1,0:T(8,128)(2,1)}, u32[]{:S(2)}) copy-start(bf16[640,1024]{1,0:T(8,128)(2,1)} %param.20) | copy-start | bytes 3932164
  15.9 108.3 %all-gather.15.cloned.1.call-start = ((), (), s32[]{:S(2)}) async-start(), calls=%async_computation.11 | async-start | bytes 7208960 | tf_op jit(solution)/shard_map/all_gather | solution.py:67
  44.1 218.6 %all-gather.9.cloned.1.call-start = ((), (), s32[]{:S(2)}) async-start(), calls=%async_computation.8 | async-start | bytes 11894784 | tf_op jit(solution)/shard_map/all_gather | solution.py:61
  45.0 373.6 %all-gather.11.cloned.1.call-start = ((), (), s32[]{:S(2)}) async-start(), calls=%async_computation.9 | async-start | bytes 4325376 | tf_op jit(solution)/shard_map/all_gather | solution.py:61
  48.4 4.8 copy-start.16
  48.4 4.8 copy-start.17
  48.4 72.9 %copy-start.9 = (f32[512,64]{0,1:T(8,128)S(1)}, f32[512,64]{0,1:T(8,128)}, u32[]{:S(2)}) copy-start(f32[512,64]{0,1:T(8,128)} %param.38) | copy-start | bytes 393220
  48.4 72.9 %all-to-all-start = ((bf16[2,640,1024]{1,2,0:T(8,128)(2,1)}), bf16[2,640,1024]{1,2,0:T(8,128)(2,1)S(1)}, u32[]{:S(2)}, u32[]{:S(2)}) async-start(bf16[2,640,1024]{1,2,0:T(8,128)(2,1)} %broadcast_in_dim.18), calls=%async_computation | async-start | bytes 5242880 | tf_op jit(solution)/shard_map/all_to_all | solution.py:29
  53.2 68.8 %copy-start.10 = (f32[2048]{0:T(1024)S(1)}, f32[2048]{0:T(1024)}, u32[]{:S(2)}) copy-start(f32[2048]{0:T(1024)} %param.21) | copy-start | bytes 24580
  124.2 138.6 %copy-start.2 = (bf16[640,2048]{0,1:T(8,128)(2,1)S(1)}, bf16[640,2048]{0,1:T(8,128)(2,1)}, u32[]{:S(2)}) copy-start(bf16[640,2048]{0,1:T(8,128)(2,1)} %fusion.5) | copy-start | bytes 7864324
  124.2 138.6 %copy-start.18 = (f32[1408]{0:T(1024)S(1)}, f32[1408]{0:T(1024)}, u32[]{:S(2)}) copy-start(f32[1408]{0:T(1024)} %param.27) | copy-start | bytes 16900
  130.0 141.5 %copy-start.19 = (f32[1408]{0:T(1024)S(1)}, f32[1408]{0:T(1024)}, u32[]{:S(2)}) copy-start(f32[1408]{0:T(1024)} %param.28) | copy-start | bytes 16900
  321.0 97.6 %copy-start.20 = (f32[512]{0:T(512)S(1)}, f32[512]{0:T(512)}, u32[]{:S(2)}) copy-start(f32[512]{0:T(512)} %param.33) | copy-start | bytes 6148
  449.6 7.3 %copy-start.14 = (f32[512]{0:T(512)S(1)}, f32[512]{0:T(512)}, u32[]{:S(2)}) copy-start(f32[512]{0:T(512)} %param.35) | copy-start | bytes 6148
  449.6 7.3 %copy-start.15 = (f32[512]{0:T(512)S(1)}, f32[512]{0:T(512)}, u32[]{:S(2)}) copy-start(f32[512]{0:T(512)} %param.34) | copy-start | bytes 6148
  449.6 34.1 %all-to-all-start.4 = ((bf16[32,512,64]{1,2,0:T(8,128)(2,1)}), bf16[32,512,64]{1,2,0:T(8,128)(2,1)}, u32[]{:S(2)}, u32[]{:S(2)}) async-start(bf16[32,512,64]{1,2,0:T(8,128)(2,1)} %broadcast_in_dim.23), calls=%async_computation.4 | async-start | bytes 4194304 | tf_op jit(solution)/shard_map/all_to_all | solution.py:29
  456.8 1.9 copy-start.6
  456.8 1.9 copy-start.13
  458.7 25.0 %copy-start.21 = (f32[512]{0:T(512)S(1)}, f32[512]{0:T(512)}, u32[]{:S(2)}) copy-start(f32[512]{0:T(512)} %param.32) | copy-start | bytes 6148
  (4 other events, 4.2 us)
Sparse Core Ops, SparseCore 0:
  16.1 27.9 all-gather.12
  45.8 61.8 all-gather.14
  109.3 153.4 all-gather.8
  264.3 154.3 all-gather.10
where the time goes:
time: 564 us; the launch traced here: 554 us
  waiting for transfers between devices  280 us (50%)
  blocking collectives  150 us (27%)
  matrix products  62.6 us (11%)
  local copies, waits for them, and re-layouts  21.1 us (4%)
  other arithmetic  15.4 us (3%)
  between operations  13.7 us (2%)
  starting transfers between devices  12.1 us (2%)
    all_gather x2, waiting for transfers between devices, sent_together(): lax.all_gather(both, axis, axis=dim, tiled=True)  228 us
    all_gather x1, blocking collectives, rows_first(): result, at, done = (lax.all_gather(both, axis, axis=0, tiled=True), 0, [])  68 us
    all_to_all x3, blocking collectives, sum_at_owner(): lax.all_to_all(parts, axis, split_axis=0, concat_axis=0, tiled=True)  38.5 us
    all_to_all x3, blocking collectives, sent_to_all(): lax.all_to_all(jnp.broadcast_to(x[None], (size, *x.shape)), axis, 0, 0, t...  35.8 us
    all_gather x2, waiting for transfers between devices, gather_in_order(): parts = lax.all_gather(parts, axes[k])  28.1 us
    all_to_all x2, waiting for transfers between devices, sent_to_all(): lax.all_to_all(jnp.broadcast_to(x[None], (size, *x.shape)), axis, 0, 0, t...  23.1 us
    dot_general x2, matrix products, hidden_units(): jnp.dot(normed, gate_all, preferred_element_type=jnp.float32) * gate_scale  17.4 us
    dot_general x1, matrix products, on_device(): jnp.dot(second_hidden, down_all, preferred_element_type=jnp.float32)  16.5 us
  transfers between devices with their start and end apart: 6, of which 4 were waited for; matrix products, arithmetic and copies ran while one was open for 8% of the time, Pallas kernels for 0%

commit v1 on v0

v1 whole, which is shorter than its diff:
```python
import functools

import jax
import jax.numpy as jnp
from jax import lax
from jax.experimental import pallas as pl
from jax.experimental.pallas import tpu as pltpu
from jax.sharding import Mesh
from jax.sharding import PartitionSpec as P

BW = 1024
SPAN = 128
EPS = 1e-06
FS = ("fs_0", "fs_1", "fs_2")
REP_FS = ("rep", "fs_0", "fs_1", "fs_2")
MESH = pl.DeviceIdType.MESH
BF = jnp.bfloat16
F32 = jnp.float32

N_UNITS = 23
NARROW = 16
ROUTES = (
    1, 0, 0, 1, 0, 3, 2, 2, 1, 2, 0, 1, 1, 3, 3, 3, 1, 0, 2, 0, 3, 0, 3,
)
PROGRAM = (
    0, 10, 20, 30, 40, 50, 60, 1090, 1, 11, 21, 31, 41, 51, 61, 70, 80, 90, 100, 110, 2, 12, 120,
    32, 22, 130, 71, 42, 140, 150, 91, 160, 52, 170, 62, 81, 101, 131, 111, 141, 151, 3, 13, 121,
    33, 23, 72, 92, 171, 43, 161, 63, 102, 53, 82, 4, 132, 112, 34, 73, 142, 93, 172, 152, 14,
    122, 24, 5, 180, 1100, 44, 54, 162, 83, 35, 190, 1103, 64, 113, 103, 123, 133, 15, 200, 1101,
    55, 210, 1105, 163, 84, 74, 191, 143, 25, 220, 1102, 114, 181, 124, 94, 45, 1104, 201, 134,
    173, 211, 153, 164, 192, 65, 1106, 85, 1108, 104, 221, 144, 75, 1107, 182, 115, 95, 1109,
    135, 212, 202, 174, 125, 193, 154, 222, 165, 145, 213, 183, 203, 194, 223, 155, 105, 1110,
    214, 1120, 1121, 1122, 1123, 1124, 1125, 204, 1126, 1127, 175, 184, 1130, 1131, 224, 185,
    1140, 195, 1141, 205, 1150, 1151, 1160, 225, 1161, 215, 1170, 1171,
)

GROUPS_OF_ROWS = ((0, 384), (384, 256))
STEP_ROWS = 32


def gelu(a):
    return 0.5 * a * (1.0 + jnp.tanh(0.7978845608028654 * (a + 0.044715 * (a * a * a))))


def silu(a):
    return 0.5 * a * (1.0 + jnp.tanh(0.5 * a))


def dot(a, b):
    return jnp.dot(a, b, preferred_element_type=F32)


def dot_t(a, b):
    return lax.dot_general(a, b, (((1,), (1,)), ((), ())), preferred_element_type=F32)


def kernel(
    tokens, norm_first, norm_mix, norm_second, gate_w, up_w, down_w, gate_s, up_s, down_s,
    u_w, v_w, u_s, v_s, ln_gain, ln_bias, spatial_w, spatial_b, out_w, out_s,
    result,
    wide, narrow, whole, normed, middle, hidden, part, got_first, got_mix, last_part, got_last,
    u_act, v_act, mixed, stats, stats_got,
    sent, arrived, pair_sent, pair_arrived,
):
    rep, z, y, x, tp = (lax.axis_index(a) for a in ("rep", "fs_0", "fs_1", "fs_2", "tp"))
    xp, xm = lax.rem(x + 1, 4), lax.rem(x + 3, 4)
    yp, ym = lax.rem(y + 1, 4), lax.rem(y + 3, 4)
    full_z = rep * 2 + z
    zp, zm = lax.rem(full_z + 1, 4), lax.rem(full_z + 3, 4)
    to_xp, to_xm = {"fs_2": xp}, {"fs_2": xm}
    to_yp, to_ym = {"fs_1": yp}, {"fs_1": ym}
    to_zp = {"rep": zp // 2, "fs_0": lax.rem(zp, 2)}
    to_zm = {"rep": zm // 2, "fs_0": lax.rem(zm, 2)}
    partner = {"tp": 1 - tp}

    def unit(u):
        return narrow if u == NARROW else wide.at[u if u < NARROW else u - 1]

    def place(u, value):
        if u == NARROW:
            narrow[z, y, x] = value.astype(BF)
        else:
            wide[u if u < NARROW else u - 1, z, y, x] = value.astype(BF)

    for i in range(11):
        cols, row = slice(128 * i, 128 * i + 128), slice(i, i + 1)
        place(i, jnp.concatenate([gate_w[:, cols] * gate_s[row], up_w[:, cols] * up_s[row]], axis=1))
    diagonal = lax.broadcasted_iota(jnp.int32, (64, 64), 0) == lax.broadcasted_iota(
        jnp.int32, (64, 64), 1)

    def upright(ref):
        return jnp.sum(jnp.where(diagonal, ref[...], 0.0), axis=1, keepdims=True)

    down_scale, out_scale = upright(down_s), upright(out_s)
    for j in range(5):
        place(11 + j, down_w[:, 256 * j : 256 * j + 256] * down_scale)
    place(NARROW, down_w[:, 1280:1408] * down_scale)
    for j in range(2):
        cols = slice(256 * j, 256 * j + 256)
        place(17 + j, v_w[:, cols] * v_s[:, cols])
        place(19 + j, u_w[:, cols] * u_s[:, cols])
        place(21 + j, out_w[:, cols] * out_scale)
    whole[tp] = tokens[...]

    barrier = pltpu.get_barrier_semaphore()
    for other in (to_xp, to_xm, to_yp, to_ym, to_zp, to_zm, partner):
        pl.semaphore_signal(barrier, inc=1, device_id=other, device_id_type=MESH)
    pl.semaphore_wait(barrier, 7)

    def send(ref, to, u, k):
        pltpu.make_async_remote_copy(
            src_ref=ref, dst_ref=ref, send_sem=sent.at[u, k], recv_sem=arrived.at[u, k],
            device_id=to, device_id_type=MESH,
        ).start()

    def region(u, k):
        b = unit(u)
        if ROUTES[u] < 2:
            return (b.at[0, 0, 0:2], b.at[0, 0, 0], b.at[0, 0:2], b.at[0, 0], b.at[0])[k]
        return (b.at[0, 0, 0], b.at[0, 0], b.at[0, 0, 0:2], b.at[0], b.at[0, 0:2])[k]

    def wait_for(u, k, sems):
        ref = region(u, k)
        pltpu.make_async_copy(ref, ref, sems.at[u, k]).wait()

    def step(u, k):
        if k > 0:
            wait_for(u, k - 1, arrived)
        b, route = unit(u), ROUTES[u]
        if k == 5:
            return
        if route == 0:
            refs = (
                ((b.at[z, y, x], to_xp), (b.at[z, y, x], to_xm)),
                ((b.at[z, y, xm, 0:32], to_xp), (b.at[z, y, xp, 32:64], to_xm)),
                ((b.at[z, y], to_yp), (b.at[z, y], to_ym)),
                ((b.at[z, ym, 0:2], to_yp), (b.at[z, yp, 2:4], to_ym)),
                ((b.at[z, 0:2], to_zp), (b.at[z, 2:4], to_zm)),
            )
        elif route == 1:
            refs = (
                ((b.at[z, y, x], to_yp), (b.at[z, y, x], to_ym)),
                ((b.at[z, ym, x, 0:32], to_yp), (b.at[z, yp, x, 32:64], to_ym)),
                ((b.at[z, :, x], to_xp), (b.at[z, :, x], to_xm)),
                ((b.at[z, 0:2, xm], to_xp), (b.at[z, 2:4, xp], to_xm)),
                ((b.at[z, 0:2], to_zp), (b.at[z, 2:4], to_zm)),
            )
        elif route == 2:
            refs = (
                ((b.at[z, y, x, 0:32], to_zp), (b.at[z, y, x, 32:64], to_zm)),
                ((b.at[:, y, x], to_xp), (b.at[:, y, x], to_xm)),
                ((b.at[0, y, xm], to_xp), (b.at[1, y, xp], to_xm)),
                ((b.at[:, y], to_yp), (b.at[:, y], to_ym)),
                ((b.at[0, ym], to_yp), (b.at[1, yp], to_ym)),
            )
        else:
            refs = (
                ((b.at[z, y, x, 0:32], to_zp), (b.at[z, y, x, 32:64], to_zm)),
                ((b.at[:, y, x], to_yp), (b.at[:, y, x], to_ym)),
                ((b.at[0, ym, x], to_yp), (b.at[1, yp, x], to_ym)),
                ((b.at[:, :, x], to_xp), (b.at[:, :, x], to_xm)),
                ((b.at[0, :, xm], to_xp), (b.at[1, :, xp], to_xm)),
            )
        for ref, to in refs[k]:
            send(ref, to, u, k)

    def pair(src, dst, n):
        return pltpu.make_async_remote_copy(
            src_ref=src, dst_ref=dst, send_sem=pair_sent.at[n], recv_sem=pair_arrived.at[n],
            device_id=partner, device_id_type=MESH,
        )

    def rows_of(h):
        at, size = GROUPS_OF_ROWS[h]
        return pl.ds(at, size)

    exchange_tokens = pair(tokens, whole.at[tp], 0)
    exchange_tokens.start()
    exchange_first = [pair(part.at[rows_of(h)], got_first.at[rows_of(h)], 1 + h) for h in (0, 1)]
    exchange_stats = [pair(stats.at[rows_of(h)], stats_got.at[rows_of(h)], 3 + h) for h in (0, 1)]
    exchange_mix = [pair(part.at[rows_of(h)], got_mix.at[rows_of(h)], 5 + h) for h in (0, 1)]
    exchange_last = [
        pair(last_part.at[rows_of(h)], got_last.at[rows_of(h)], 7 + h) for h in (0, 1)
    ]

    def by_rows(at, size, step_rows, body):
        def one(i, carry):
            body(pl.ds(pl.multiple_of(at + i * step_rows, step_rows), step_rows))
            return carry

        lax.fori_loop(0, size // step_rows, one, 0)

    def normalise(values, gain):
        factor = lax.rsqrt(jnp.mean(values * values, axis=1, keepdims=True) + EPS)
        return (values * factor * gain[...]).astype(BF)

    def norm_tokens():
        exchange_tokens.wait()

        def body(r):
            values = jnp.concatenate([whole[0, r], whole[1, r]], axis=1).astype(F32)
            normed[r] = normalise(values, norm_first)

        by_rows(0, 640, STEP_ROWS, body)

    def gate_up(u, at, size):
        r = pl.ds(at, size)
        both = dot(normed[r], wide[u].reshape(2048, 256))
        hidden[u, r] = (silu(both[:, :128]) * both[:, 128:]).astype(BF)

    def first_hidden(u):
        def one(i, carry):
            gate_up(u, pl.multiple_of(i * 320, 320), 320)
            return carry

        lax.fori_loop(0, 2, one, 0)

    def down_rows(h, zi, yi):
        r = rows_of(h)
        left = jnp.concatenate([hidden[i, r] for i in range(11)], axis=1)
        right = jnp.concatenate(
            [wide[11 + j, zi, pl.ds(yi, 2)].reshape(512, 256) for j in range(5)]
            + [narrow[zi, pl.ds(yi, 2)].reshape(512, 128)], axis=1)
        return dot_t(left, right)

    def first_down(h, nb):
        part[rows_of(h), 512 * nb : 512 * nb + 512] = down_rows(h, nb // 2, 2 * (nb % 2)).astype(BF)
        if nb == 3:
            exchange_first[h].start()

    def combine_first(h):
        exchange_first[h].wait()

        def body(r):
            values = jnp.concatenate([whole[0, r], whole[1, r]], axis=1).astype(F32)
            branch = part[r].astype(F32) + got_first[r].astype(F32)
            total = (values + 0.5 * branch).astype(BF)
            middle[r] = total
            normed[r] = normalise(total.astype(F32), norm_mix)

        by_rows(*GROUPS_OF_ROWS[h], STEP_ROWS, body)

    def project_v(h):
        r = rows_of(h)
        lane = lax.broadcasted_iota(jnp.int32, (GROUPS_OF_ROWS[h][1], 128), 1)
        total = total_sq = 0.0
        for j in range(2):
            act = gelu(dot(normed[r], wide[16 + j].reshape(2048, 256)))
            v_act[r, 256 * j : 256 * j + 256] = act
            total += jnp.sum(act, axis=1, keepdims=True)
            total_sq += jnp.sum(act * act, axis=1, keepdims=True)
        stats[r] = jnp.where(lane == 0, total, jnp.where(lane == 1, total_sq, 0.0))
        exchange_stats[h].start()

    def project_u(h):
        r = rows_of(h)
        for j in range(2):
            act = gelu(dot(normed[r], wide[18 + j].reshape(2048, 256)))
            u_act[r, 256 * j : 256 * j + 256] = act

    def mix(h):
        exchange_stats[h].wait()
        row = lax.broadcasted_iota(jnp.int32, (SPAN, SPAN), 0)
        col = lax.broadcasted_iota(jnp.int32, (SPAN, SPAN), 1)

        def body(r):
            sums = stats[r] + stats_got[r]
            mean = sums[:, 0:1] * (1.0 / BW)
            var = sums[:, 1:2] * (1.0 / BW) - mean * mean
            factor = lax.rsqrt(var + EPS)
            for g in range(4):
                c = slice(128 * g, 128 * g + 128)
                v = ((v_act[r, c] - mean) * factor * ln_gain[:, c] + ln_bias[:, c]).astype(BF)
                w = jnp.where(col <= row, spatial_w[g].astype(F32), 0.0).astype(BF)
                bias = jnp.sum(
                    jnp.where(col == row, spatial_b[g : g + 1, :], 0.0), axis=1, keepdims=True)
                spatial = dot(w, v) + bias
                mixed[r, c] = (u_act[r, c] * spatial).astype(BF)

        by_rows(*GROUPS_OF_ROWS[h], SPAN, body)

    def project_out(h):
        r = rows_of(h)

        def one(nb, carry):
            zi, yi = nb // 2, 2 * lax.rem(nb, 2)
            right = jnp.concatenate(
                [wide[20 + j, zi, pl.ds(yi, 2)].reshape(512, 256) for j in range(2)], axis=1)
            cols = pl.ds(pl.multiple_of(512 * nb, 512), 512)
            part[r, cols] = dot_t(mixed[r], right).astype(BF)
            return carry

        lax.fori_loop(0, 4, one, 0)
        exchange_mix[h].start()

    def combine_mix(h):
        exchange_mix[h].wait()

        def body(r):
            branch = part[r].astype(F32) + got_mix[r].astype(F32)
            total = (middle[r].astype(F32) + branch).astype(BF)
            middle[r] = total
            normed[r] = normalise(total.astype(F32), norm_second)

        by_rows(*GROUPS_OF_ROWS[h], STEP_ROWS, body)

    def second_hidden(h):
        at, size = GROUPS_OF_ROWS[h]

        def one(u, carry):
            gate_up(u, at, size)
            return carry

        lax.fori_loop(0, 11, one, 0)

    def second_down(h):
        r = rows_of(h)
        for nb in range(2):
            c = slice(512 * nb, 512 * nb + 512)
            last_part[r, c] = down_rows(h, 1 - tp, 2 * nb).astype(BF)
        exchange_last[h].start()
        for nb in range(2):
            c = slice(512 * nb, 512 * nb + 512)
            part[r, c] = down_rows(h, tp, 2 * nb).astype(BF)

    def finish(h):
        exchange_last[h].wait()

        def body(r):
            own = middle[r, pl.ds(pl.multiple_of(tp * 1024, 1024), 1024)].astype(F32)
            branch = part[r, 0:1024].astype(F32) + got_last[r].astype(F32)
            result[r] = (own + 0.5 * branch).astype(BF)

        by_rows(*GROUPS_OF_ROWS[h], STEP_ROWS, body)

    def task(n):
        if n == 90:
            norm_tokens()
        elif n < 120:
            first_hidden(n - 100)
        elif n < 130:
            first_down((n - 120) // 4, n % 4)
        else:
            run = (combine_first, project_v, project_u, mix, project_out)
            run[n // 10 - 13](n % 10)

    for code in PROGRAM:
        if code < 1000:
            step(code // 10, code % 10)
        else:
            task(code - 1000)
    for h in (0, 1):
        combine_mix(h)
        second_hidden(h)
        second_down(h)
    for h in (0, 1):
        finish(h)
    for u in range(N_UNITS):
        for k in range(5):
            wait_for(u, k, sent)


def on_device(*args):
    (tokens, norm_first, norm_mix, norm_second, gate_w, up_w, down_w, gate_s, up_s, down_s,
     u_w, v_w, u_s, v_s, ln_gain, ln_bias, spatial_w, spatial_b, out_w, out_s) = args
    line = lambda a: a.reshape(1, -1)
    rows = tokens.shape[0]
    vmem = pltpu.VMEM
    return pl.pallas_call(
        kernel,
        out_shape=jax.ShapeDtypeStruct(tokens.shape, BF),
        in_specs=[pl.BlockSpec(memory_space=pltpu.VMEM)] * 20,
        out_specs=pl.BlockSpec(memory_space=pltpu.VMEM),
        scratch_shapes=[
            vmem((N_UNITS - 1, 2, 4, 4, 64, 256), BF),
            vmem((2, 4, 4, 64, 128), BF),
            vmem((2, rows, 1024), BF),
            vmem((rows, 2048), BF),
            vmem((rows, 2048), BF),
            vmem((11, rows, 128), BF),
            vmem((rows, 2048), BF),
            vmem((rows, 2048), BF),
            vmem((rows, 2048), BF),
            vmem((rows, 1024), BF),
            vmem((rows, 1024), BF),
            vmem((rows, 512), F32),
            vmem((rows, 512), F32),
            vmem((rows, 512), BF),
            vmem((rows, 128), F32),
            vmem((rows, 128), F32),
            pltpu.SemaphoreType.DMA((N_UNITS, 5)),
            pltpu.SemaphoreType.DMA((N_UNITS, 5)),
            pltpu.SemaphoreType.DMA((9,)),
            pltpu.SemaphoreType.DMA((9,)),
        ],
        compiler_params=pltpu.CompilerParams(
            collective_id=0, has_side_effects=True, vmem_limit_bytes=67043328
        ),
    )(tokens, line(norm_first), line(norm_mix), line(norm_second), gate_w, up_w, down_w.T,
      gate_s.reshape(-1, 128), up_s.reshape(-1, 128), line(down_s), u_w, v_w, line(u_s), line(v_s), line(ln_gain),
      line(ln_bias), spatial_w, spatial_b, out_w.T, line(out_s))


def solution(mesh):
    torus = Mesh(
        mesh.devices.reshape(mesh.shape["rep"], 2, 4, 4, mesh.shape["tp"]),
        ("rep", "fs_0", "fs_1", "fs_2", "tp"),
    )
    in_specs = (
        P(REP_FS, "tp"), P(), P(), P(), P(FS, "tp"), P(FS, "tp"), P("tp", FS), P("tp"), P("tp"),
        P(FS), P(FS, "tp"), P(FS, "tp"), P("tp"), P("tp"), P("tp"), P("tp"),
        P("tp", None, None), P("tp", None), P("tp", FS), P(FS),
    )
    return jax.shard_map(
        on_device, mesh=torus, in_specs=in_specs, out_specs=P(REP_FS, "tp"), check_vma=False
    )
```

time: 564 us -> 139 us (0.25); the launches traced: 554 us -> 139 us
  waiting for transfers between devices: 280 us -> 0 us
  blocking collectives: 150 us -> 0 us
  Pallas kernels: 0 us -> 137 us
  matrix products: 62.6 us -> 0 us
  local copies, waits for them, and re-layouts: 21.1 us -> 2.47 us
  other arithmetic: 15.4 us -> 0 us
  between operations: 13.7 us -> 0.01 us
  starting transfers between devices: 12.1 us -> 0 us
    all_gather x4 -> x0, waiting for transfers between devices: 256 us -> none  [the longest x2 228 us: sent_together(): lax.all_gather(both, axis, axis=dim, tiled=True)]
    pallas_call x0 -> x1, Pallas kernels: none -> 137 us  [on_device(): pl.pallas_call(kernel, out_shape=jax.ShapeDtypeStruct(tokens.shape, BF),...]
    all_gather x2 -> x0, blocking collectives: 75.5 us -> none  [the longest x1 68 us: rows_first(): result, at, done = (lax.all_gather(both, axis, axis=0, tiled=True), 0, [])]
    all_to_all x6 -> x0, blocking collectives: 74.3 us -> none  [the longest x3 38.5 us: sum_at_owner(): lax.all_to_all(parts, axis, split_axis=0, concat_axis=0, tiled=True)]
    dot_general x7 -> x0, matrix products: 62.6 us -> none  [the longest x2 17.4 us: hidden_units(): jnp.dot(normed, gate_all, preferred_element_type=jnp.float32) * gate_scale]
    all_to_all x2 -> x0, waiting for transfers between devices: 23.1 us -> none  [sent_to_all(): lax.all_to_all(jnp.broadcast_to(x[None], (size, *x.shape)), axis, 0, 0, t...]
    all_to_all x2 -> x0, starting transfers between devices: 12 us -> none  [sent_to_all(): lax.all_to_all(jnp.broadcast_to(x[None], (size, *x.shape)), axis, 0, 0, t...]
    convert_element_type x13 -> x0, other arithmetic: 10.4 us -> none  [the longest x3 5.03 us: full_norm(): return (values * factor * gain).astype(jnp.bfloat16)]
  transfers between devices with their start and end apart: 6 -> 0, of which waited for: 4 -> 0; matrix products, arithmetic and copies ran while one was open for 8% -> 0% of each run, Pallas kernels for 0% -> 0%
where the time goes in v1:
time: 139 us
  Pallas kernels  137 us (99%)
  local copies, waits for them, and re-layouts  2.47 us (2%)
    pallas_call x1, Pallas kernels, on_device(): pl.pallas_call(kernel, out_shape=jax.ShapeDtypeStruct(tokens.shape, BF),...  137 us

profile of v1, /device:TPU:1, one launch (start us, length us, event | category | flops | bytes accessed | tf_op | source)
XLA Modules:
  0.0 139.1 jit_solution(10552412768216194153)
XLA Ops:
  0.0 136.6 %shard_map.190 = bf16[640,1024]{1,0:T(8,128)(2,1)} custom-call(bf16[640,1024]{1,0:T(8,128)(2,1)} %tokens.1, f32[1,2048]{1,0:T(1,128)} %bitcast.15, f32[1,2048]{1,0:T(1,128)} %bitcast.16, f32[1,2048]{1,0:T(1,128)} %bitcast.17, f32[64,1408]{1,0:T(8,128)} %gate_w.1, f32[64,1408]{1,0:T(8,128)} %up_w.1, f32[64,1408]{1,0:T(8,128)} %bitcast.13, ...), custom_call_target="tpu_custom_call" | custom-call | tf_op jit(solution)/shard_map/pallas_call | solution.py:369
  136.6 2.5 %copy.22 = bf16[640,1024]{1,0:T(8,128)(2,1)} copy(bf16[640,1024]{1,0:T(8,128)(2,1)} %shard_map.190) | data formatting | bytes 2621440

commit v2 on v1

--- a/solution.py
+++ b/solution.py
@@ -20,22 +20,24 @@
 N_UNITS = 23
 NARROW = 16
 ROUTES = (
-    1, 0, 0, 1, 0, 3, 2, 2, 1, 2, 0, 1, 1, 3, 3, 3, 1, 0, 2, 0, 3, 0, 3,
+    0, 0, 4, 1, 5, 5, 1, 2, 1, 0, 1, 4, 1, 4, 4, 5, 0, 1, 1, 2, 3, 5, 2,
 )
 PROGRAM = (
-    0, 10, 20, 30, 40, 50, 60, 1090, 1, 11, 21, 31, 41, 51, 61, 70, 80, 90, 100, 110, 2, 12, 120,
-    32, 22, 130, 71, 42, 140, 150, 91, 160, 52, 170, 62, 81, 101, 131, 111, 141, 151, 3, 13, 121,
-    33, 23, 72, 92, 171, 43, 161, 63, 102, 53, 82, 4, 132, 112, 34, 73, 142, 93, 172, 152, 14,
-    122, 24, 5, 180, 1100, 44, 54, 162, 83, 35, 190, 1103, 64, 113, 103, 123, 133, 15, 200, 1101,
-    55, 210, 1105, 163, 84, 74, 191, 143, 25, 220, 1102, 114, 181, 124, 94, 45, 1104, 201, 134,
-    173, 211, 153, 164, 192, 65, 1106, 85, 1108, 104, 221, 144, 75, 1107, 182, 115, 95, 1109,
-    135, 212, 202, 174, 125, 193, 154, 222, 165, 145, 213, 183, 203, 194, 223, 155, 105, 1110,
-    214, 1120, 1121, 1122, 1123, 1124, 1125, 204, 1126, 1127, 175, 184, 1130, 1131, 224, 185,
-    1140, 195, 1141, 205, 1150, 1151, 1160, 225, 1161, 215, 1170, 1171,
+    60, 90, 100, 150, 0, 40, 160, 130, 61, 80, 91, 50, 101, 20, 10, 151, 1, 140, 161, 120, 41,
+    1090, 62, 92, 131, 81, 51, 21, 102, 30, 11, 152, 70, 2, 170, 121, 110, 141, 162, 42, 153, 71,
+    63, 93, 132, 82, 22, 52, 43, 31, 103, 133, 12, 3, 111, 142, 171, 23, 122, 53, 163, 94, 143,
+    32, 154, 72, 64, 134, 95, 180, 1109, 83, 13, 4, 172, 65, 190, 1106, 44, 104, 112, 24, 164,
+    123, 5, 220, 1100, 191, 144, 54, 105, 210, 1110, 135, 200, 181, 113, 33, 14, 165, 155, 221,
+    201, 73, 25, 1102, 84, 145, 211, 182, 173, 15, 1101, 45, 1104, 124, 114, 192, 85, 1108, 202,
+    55, 1105, 34, 222, 125, 74, 212, 183, 174, 115, 193, 203, 223, 35, 1103, 184, 75, 1107, 213,
+    1120, 1121, 1122, 1123, 1124, 1125, 1126, 204, 1127, 194, 175, 1130, 1131, 214, 224, 185,
+    1140, 1141, 205, 195, 1150, 1151, 1160, 215, 1161, 225, 1170, 1171,
 )
 
 GROUPS_OF_ROWS = ((0, 384), (384, 256))
-STEP_ROWS = 32
+STEP_ROWS = 16
+UNROLL = 8
+PLACED_AHEAD = 4
 
 
 def gelu(a):
@@ -55,12 +57,13 @@
 
 
 def kernel(
-    tokens, norm_first, norm_mix, norm_second, gate_w, up_w, down_w, gate_s, up_s, down_s,
-    u_w, v_w, u_s, v_s, ln_gain, ln_bias, spatial_w, spatial_b, out_w, out_s,
+    tokens, norm_first, norm_mix, norm_second, gate_hbm, up_hbm, down_hbm, gate_s, up_s, down_s,
+    u_hbm, v_hbm, u_s, v_s, ln_gain, ln_bias, spatial_w, spatial_b, out_hbm, out_s,
     result,
+    gate_w, up_w, down_w, v_w, u_w, out_w,
     wide, narrow, whole, normed, middle, hidden, part, got_first, got_mix, last_part, got_last,
     u_act, v_act, mixed, stats, stats_got,
-    sent, arrived, pair_sent, pair_arrived,
+    sent, arrived, pair_sent, pair_arrived, load_sem, store_sem,
 ):
     rep, z, y, x, tp = (lax.axis_index(a) for a in ("rep", "fs_0", "fs_1", "fs_2", "tp"))
     xp, xm = lax.rem(x + 1, 4), lax.rem(x + 3, 4)
@@ -76,35 +79,62 @@
     def unit(u):
         return narrow if u == NARROW else wide.at[u if u < NARROW else u - 1]
 
-    def place(u, value):
-        if u == NARROW:
-            narrow[z, y, x] = value.astype(BF)
-        else:
-            wide[u if u < NARROW else u - 1, z, y, x] = value.astype(BF)
-
-    for i in range(11):
-        cols, row = slice(128 * i, 128 * i + 128), slice(i, i + 1)
-        place(i, jnp.concatenate([gate_w[:, cols] * gate_s[row], up_w[:, cols] * up_s[row]], axis=1))
-    diagonal = lax.broadcasted_iota(jnp.int32, (64, 64), 0) == lax.broadcasted_iota(
-        jnp.int32, (64, 64), 1)
-
-    def upright(ref):
-        return jnp.sum(jnp.where(diagonal, ref[...], 0.0), axis=1, keepdims=True)
-
-    down_scale, out_scale = upright(down_s), upright(out_s)
-    for j in range(5):
-        place(11 + j, down_w[:, 256 * j : 256 * j + 256] * down_scale)
-    place(NARROW, down_w[:, 1280:1408] * down_scale)
-    for j in range(2):
-        cols = slice(256 * j, 256 * j + 256)
-        place(17 + j, v_w[:, cols] * v_s[:, cols])
-        place(19 + j, u_w[:, cols] * u_s[:, cols])
-        place(21 + j, out_w[:, cols] * out_scale)
-    whole[tp] = tokens[...]
-
     barrier = pltpu.get_barrier_semaphore()
     for other in (to_xp, to_xm, to_yp, to_ym, to_zp, to_zm, partner):
         pl.semaphore_signal(barrier, inc=1, device_id=other, device_id_type=MESH)
+
+    loads = {}
+    for n, (name, source, target) in enumerate((
+        ("gate", gate_hbm, gate_w), ("up", up_hbm, up_w), ("down", down_hbm, down_w),
+        ("v", v_hbm, v_w), ("u", u_hbm, u_w), ("out", out_hbm, out_w),
+        ("tokens", tokens, whole.at[tp]),
+    )):
+        loads[name] = pltpu.make_async_copy(source, target, load_sem.at[n])
+        loads[name].start()
+    loaded = set()
+
+    def need(*names):
+        for name in names:
+            if name not in loaded:
+                loaded.add(name)
+                loads[name].wait()
+
+    diagonal = lax.broadcasted_iota(jnp.int32, (64, 64), 0) == lax.broadcasted_iota(
+        jnp.int32, (64, 64), 1)
+
+    def upright(ref):
+        return jnp.sum(jnp.where(diagonal, ref[...], 0.0), axis=1, keepdims=True)
+
+    def place(u):
+        if u < 11:
+            need("gate", "up")
+            cols, row = slice(128 * u, 128 * u + 128), slice(u, u + 1)
+            wide[u, z, y, x] = jnp.concatenate(
+                [gate_w[:, cols] * gate_s[row], up_w[:, cols] * up_s[row]], axis=1).astype(BF)
+        elif u < NARROW:
+            need("down")
+            at = 256 * (u - 11)
+            wide[u, z, y, x] = (down_w[:, at : at + 256] * upright(down_s)).astype(BF)
+        elif u == NARROW:
+            need("down")
+            narrow[z, y, x] = (down_w[:, 1280:1408] * upright(down_s)).astype(BF)
+        else:
+            at = 256 * ((u - 17) % 2)
+            cols = slice(at, at + 256)
+            if u < 19:
+                need("v")
+                value = v_w[:, cols] * v_s[:, cols]
+            elif u < 21:
+                need("u")
+                value = u_w[:, cols] * u_s[:, cols]
+            else:
+                need("out")
+                value = out_w[:, cols] * upright(out_s)
+            wide[u - 1, z, y, x] = value.astype(BF)
+
+    to_place = [code // 10 for code in PROGRAM if code < 1000 and code % 10 == 0]
+    for _ in range(PLACED_AHEAD):
+        place(to_place.pop(0))
     pl.semaphore_wait(barrier, 7)
 
     def send(ref, to, u, k):
@@ -117,7 +147,9 @@
         b = unit(u)
         if ROUTES[u] < 2:
             return (b.at[0, 0, 0:2], b.at[0, 0, 0], b.at[0, 0:2], b.at[0, 0], b.at[0])[k]
-        return (b.at[0, 0, 0], b.at[0, 0], b.at[0, 0, 0:2], b.at[0], b.at[0, 0:2])[k]
+        if ROUTES[u] < 4:
+            return (b.at[0, 0, 0], b.at[0, 0], b.at[0, 0, 0:2], b.at[0], b.at[0, 0:2])[k]
+        return (b.at[0, 0, 0:2], b.at[0, 0, 0], b.at[0, 0], b.at[0], b.at[0, 0:2])[k]
 
     def wait_for(u, k, sems):
         ref = region(u, k)
@@ -126,6 +158,8 @@
     def step(u, k):
         if k > 0:
             wait_for(u, k - 1, arrived)
+        elif to_place:
+            place(to_place.pop(0))
         b, route = unit(u), ROUTES[u]
         if k == 5:
             return
@@ -153,11 +187,27 @@
                 ((b.at[:, y], to_yp), (b.at[:, y], to_ym)),
                 ((b.at[0, ym], to_yp), (b.at[1, yp], to_ym)),
             )
-        else:
+        elif route == 3:
             refs = (
                 ((b.at[z, y, x, 0:32], to_zp), (b.at[z, y, x, 32:64], to_zm)),
                 ((b.at[:, y, x], to_yp), (b.at[:, y, x], to_ym)),
                 ((b.at[0, ym, x], to_yp), (b.at[1, yp, x], to_ym)),
+                ((b.at[:, :, x], to_xp), (b.at[:, :, x], to_xm)),
+                ((b.at[0, :, xm], to_xp), (b.at[1, :, xp], to_xm)),
+            )
+        elif route == 4:
+            refs = (
+                ((b.at[z, y, x], to_xp), (b.at[z, y, x], to_xm)),
+                ((b.at[z, y, xm, 0:32], to_xp), (b.at[z, y, xp, 32:64], to_xm)),
+                ((b.at[z, y, 0:2], to_zp), (b.at[z, y, 2:4], to_zm)),
+                ((b.at[:, y], to_yp), (b.at[:, y], to_ym)),
+                ((b.at[0, ym], to_yp), (b.at[1, yp], to_ym)),
+            )
+        else:
+            refs = (
+                ((b.at[z, y, x], to_yp), (b.at[z, y, x], to_ym)),
+                ((b.at[z, ym, x, 0:32], to_yp), (b.at[z, yp, x, 32:64], to_ym)),
+                ((b.at[z, 0:2, x], to_zp), (b.at[z, 2:4, x], to_zm)),
                 ((b.at[:, :, x], to_xp), (b.at[:, :, x], to_xm)),
                 ((b.at[0, :, xm], to_xp), (b.at[1, :, xp], to_xm)),
             )
@@ -183,18 +233,24 @@
         pair(last_part.at[rows_of(h)], got_last.at[rows_of(h)], 7 + h) for h in (0, 1)
     ]
 
+    stores = [
+        pltpu.make_async_copy(last_part.at[rows_of(h)], result.at[rows_of(h)], store_sem.at[h])
+        for h in (0, 1)
+    ]
+
     def by_rows(at, size, step_rows, body):
         def one(i, carry):
             body(pl.ds(pl.multiple_of(at + i * step_rows, step_rows), step_rows))
             return carry
 
-        lax.fori_loop(0, size // step_rows, one, 0)
+        lax.fori_loop(0, size // step_rows, one, 0, unroll=UNROLL if step_rows < SPAN else 1)
 
     def normalise(values, gain):
         factor = lax.rsqrt(jnp.mean(values * values, axis=1, keepdims=True) + EPS)
         return (values * factor * gain[...]).astype(BF)
 
     def norm_tokens():
+        need("tokens")
         exchange_tokens.wait()
 
         def body(r):
@@ -203,17 +259,12 @@
 
         by_rows(0, 640, STEP_ROWS, body)
 
-    def gate_up(u, at, size):
-        r = pl.ds(at, size)
-        both = dot(normed[r], wide[u].reshape(2048, 256))
-        hidden[u, r] = (silu(both[:, :128]) * both[:, 128:]).astype(BF)
+    def activate(both):
+        return (silu(both[:, :128]) * both[:, 128:]).astype(BF)
 
     def first_hidden(u):
-        def one(i, carry):
-            gate_up(u, pl.multiple_of(i * 320, 320), 320)
-            return carry
-
-        lax.fori_loop(0, 2, one, 0)
+        for r in (pl.ds(0, 320), pl.ds(320, 320)):
+            hidden[u, r] = activate(dot(normed[r], wide[u].reshape(2048, 256)))
 
     def down_rows(h, zi, yi):
         r = rows_of(h)
@@ -282,15 +333,11 @@
     def project_out(h):
         r = rows_of(h)
 
-        def one(nb, carry):
-            zi, yi = nb // 2, 2 * lax.rem(nb, 2)
+        for nb in range(4):
             right = jnp.concatenate(
-                [wide[20 + j, zi, pl.ds(yi, 2)].reshape(512, 256) for j in range(2)], axis=1)
-            cols = pl.ds(pl.multiple_of(512 * nb, 512), 512)
-            part[r, cols] = dot_t(mixed[r], right).astype(BF)
-            return carry
-
-        lax.fori_loop(0, 4, one, 0)
+                [wide[20 + j, nb // 2, pl.ds(2 * (nb % 2), 2)].reshape(512, 256) for j in range(2)],
+                axis=1)
+            part[r, 512 * nb : 512 * nb + 512] = dot_t(mixed[r], right).astype(BF)
         exchange_mix[h].start()
 
     def combine_mix(h):
@@ -305,13 +352,13 @@
         by_rows(*GROUPS_OF_ROWS[h], STEP_ROWS, body)
 
     def second_hidden(h):
-        at, size = GROUPS_OF_ROWS[h]
-
-        def one(u, carry):
-            gate_up(u, at, size)
-            return carry
-
-        lax.fori_loop(0, 11, one, 0)
+        r = rows_of(h)
+
+        def product(u):
+            return dot(normed[r], wide[u].reshape(2048, 256))
+
+        for u in range(11):
+            hidden[u, r] = activate(product(u))
 
     def second_down(h):
         r = rows_of(h)
@@ -329,9 +376,10 @@
         def body(r):
             own = middle[r, pl.ds(pl.multiple_of(tp * 1024, 1024), 1024)].astype(F32)
             branch = part[r, 0:1024].astype(F32) + got_last[r].astype(F32)
-            result[r] = (own + 0.5 * branch).astype(BF)
+            last_part[r] = (own + 0.5 * branch).astype(BF)
 
         by_rows(*GROUPS_OF_ROWS[h], STEP_ROWS, body)
+        stores[h].start()
 
     def task(n):
         if n == 90:
@@ -358,6 +406,8 @@
     for u in range(N_UNITS):
         for k in range(5):
             wait_for(u, k, sent)
+    for store in stores:
+        store.wait()
 
 
 def on_device(*args):
@@ -369,9 +419,14 @@
     return pl.pallas_call(
         kernel,
         out_shape=jax.ShapeDtypeStruct(tokens.shape, BF),
-        in_specs=[pl.BlockSpec(memory_space=pltpu.VMEM)] * 20,
-        out_specs=pl.BlockSpec(memory_space=pltpu.VMEM),
+        in_specs=[
+            pl.BlockSpec(memory_space=pl.ANY if n in (0, 4, 5, 6, 10, 11, 18) else pltpu.VMEM)
+            for n in range(20)
+        ],
+        out_specs=pl.BlockSpec(memory_space=pl.ANY),
         scratch_shapes=[
+            *[vmem((64, 1408), F32)] * 3,
+            *[vmem((64, 512), F32)] * 3,
             vmem((N_UNITS - 1, 2, 4, 4, 64, 256), BF),
             vmem((2, 4, 4, 64, 128), BF),
             vmem((2, rows, 1024), BF),
@@ -390,8 +445,7 @@
             vmem((rows, 128), F32),
             pltpu.SemaphoreType.DMA((N_UNITS, 5)),
             pltpu.SemaphoreType.DMA((N_UNITS, 5)),
-            pltpu.SemaphoreType.DMA((9,)),
-            pltpu.SemaphoreType.DMA((9,)),
+            *[pltpu.SemaphoreType.DMA((n,)) for n in (9, 9, 7, 2)],
         ],
         compiler_params=pltpu.CompilerParams(
             collective_id=0, has_side_effects=True, vmem_limit_bytes=67043328

time: 139 us -> 126 us (0.906)
  Pallas kernels: 137 us -> 123 us
    pallas_call x1, Pallas kernels: 137 us -> 123 us  [on_device(): pl.pallas_call(kernel, out_shape=jax.ShapeDtypeStruct(tokens.shape, BF),...]
where the time goes in v2:
time: 126 us; the launch traced here: 125 us
  Pallas kernels  123 us (98%)
  local copies, waits for them, and re-layouts  2.47 us (2%)
    pallas_call x1, Pallas kernels, on_device(): pl.pallas_call(kernel, out_shape=jax.ShapeDtypeStruct(tokens.shape, BF),...  123 us

profile of v2, /device:TPU:1, one launch (start us, length us, event | category | flops | bytes accessed | tf_op | source)
XLA Modules:
  0.0 125.4 jit_solution(2311466926764484154)
XLA Ops:
  0.0 122.9 %shard_map.190 = bf16[640,1024]{1,0:T(8,128)(2,1)} custom-call(bf16[640,1024]{1,0:T(8,128)(2,1)} %tokens.1, f32[1,2048]{1,0:T(1,128)} %bitcast.15, f32[1,2048]{1,0:T(1,128)} %bitcast.16, f32[1,2048]{1,0:T(1,128)} %bitcast.17, f32[64,1408]{1,0:T(8,128)} %gate_hbm.1, f32[64,1408]{1,0:T(8,128)} %up_hbm.1, f32[64,1408]{1,0:T(8,128)} %bitcast.13, ...), custom_call_target="tpu_custom_call" | custom-call | tf_op jit(solution)/shard_map/pallas_call | solution.py:419
  122.9 2.5 %copy.22 = bf16[640,1024]{1,0:T(8,128)(2,1)} copy(bf16[640,1024]{1,0:T(8,128)(2,1)} %shard_map.190) | data formatting | bytes 2621440

commit v3 on v2

--- a/solution.py
+++ b/solution.py
@@ -57,9 +57,12 @@
 
 
 def kernel(
-    tokens, norm_first, norm_mix, norm_second, gate_hbm, up_hbm, down_hbm, gate_s, up_s, down_s,
-    u_hbm, v_hbm, u_s, v_s, ln_gain, ln_bias, spatial_w, spatial_b, out_hbm, out_s,
+    tokens, norm_first_hbm, norm_mix_hbm, norm_second_hbm, gate_hbm, up_hbm, down_hbm,
+    gate_s_hbm, up_s_hbm, down_s_hbm, u_hbm, v_hbm, u_s_hbm, v_s_hbm, ln_gain_hbm, ln_bias_hbm,
+    spatial_w_hbm, spatial_b_hbm, out_hbm, out_s_hbm,
     result,
+    norm_first, norm_mix, norm_second, gate_s, up_s, down_s, u_s, v_s, ln_gain, ln_bias,
+    spatial_w, spatial_b, out_s,
     gate_w, up_w, down_w, v_w, u_w, out_w,
     wide, narrow, whole, normed, middle, hidden, part, got_first, got_mix, last_part, got_last,
     u_act, v_act, mixed, stats, stats_got,
@@ -85,9 +88,14 @@
 
     loads = {}
     for n, (name, source, target) in enumerate((
+        ("gate_s", gate_s_hbm, gate_s), ("up_s", up_s_hbm, up_s), ("down_s", down_s_hbm, down_s),
         ("gate", gate_hbm, gate_w), ("up", up_hbm, up_w), ("down", down_hbm, down_w),
+        ("v_s", v_s_hbm, v_s), ("u_s", u_s_hbm, u_s), ("out_s", out_s_hbm, out_s),
         ("v", v_hbm, v_w), ("u", u_hbm, u_w), ("out", out_hbm, out_w),
-        ("tokens", tokens, whole.at[tp]),
+        ("first", norm_first_hbm, norm_first), ("tokens", tokens, whole.at[tp]),
+        ("mix", norm_mix_hbm, norm_mix), ("second", norm_second_hbm, norm_second),
+        ("gain", ln_gain_hbm, ln_gain), ("bias", ln_bias_hbm, ln_bias),
+        ("spatial_w", spatial_w_hbm, spatial_w), ("spatial_b", spatial_b_hbm, spatial_b),
     )):
         loads[name] = pltpu.make_async_copy(source, target, load_sem.at[n])
         loads[name].start()
@@ -107,28 +115,28 @@
 
     def place(u):
         if u < 11:
-            need("gate", "up")
+            need("gate", "up", "gate_s", "up_s")
             cols, row = slice(128 * u, 128 * u + 128), slice(u, u + 1)
             wide[u, z, y, x] = jnp.concatenate(
                 [gate_w[:, cols] * gate_s[row], up_w[:, cols] * up_s[row]], axis=1).astype(BF)
         elif u < NARROW:
-            need("down")
+            need("down", "down_s")
             at = 256 * (u - 11)
             wide[u, z, y, x] = (down_w[:, at : at + 256] * upright(down_s)).astype(BF)
         elif u == NARROW:
-            need("down")
+            need("down", "down_s")
             narrow[z, y, x] = (down_w[:, 1280:1408] * upright(down_s)).astype(BF)
         else:
             at = 256 * ((u - 17) % 2)
             cols = slice(at, at + 256)
             if u < 19:
-                need("v")
+                need("v", "v_s")
                 value = v_w[:, cols] * v_s[:, cols]
             elif u < 21:
-                need("u")
+                need("u", "u_s")
                 value = u_w[:, cols] * u_s[:, cols]
             else:
-                need("out")
+                need("out", "out_s")
                 value = out_w[:, cols] * upright(out_s)
             wide[u - 1, z, y, x] = value.astype(BF)
 
@@ -220,6 +228,9 @@
             device_id=partner, device_id_type=MESH,
         )
 
+    def columns(n):
+        return [pl.ds(512 * i, 512) for i in range(n)]
+
     def rows_of(h):
         at, size = GROUPS_OF_ROWS[h]
         return pl.ds(at, size)
@@ -228,9 +239,13 @@
     exchange_tokens.start()
     exchange_first = [pair(part.at[rows_of(h)], got_first.at[rows_of(h)], 1 + h) for h in (0, 1)]
     exchange_stats = [pair(stats.at[rows_of(h)], stats_got.at[rows_of(h)], 3 + h) for h in (0, 1)]
-    exchange_mix = [pair(part.at[rows_of(h)], got_mix.at[rows_of(h)], 5 + h) for h in (0, 1)]
+    exchange_mix = [
+        [pair(part.at[rows_of(h), c], got_mix.at[rows_of(h), c], 5 + 4 * h + i)
+         for i, c in enumerate(columns(4))] for h in (0, 1)
+    ]
     exchange_last = [
-        pair(last_part.at[rows_of(h)], got_last.at[rows_of(h)], 7 + h) for h in (0, 1)
+        [pair(last_part.at[rows_of(h), c], got_last.at[rows_of(h), c], 13 + 2 * h + i)
+         for i, c in enumerate(columns(2))] for h in (0, 1)
     ]
 
     stores = [
@@ -250,7 +265,7 @@
         return (values * factor * gain[...]).astype(BF)
 
     def norm_tokens():
-        need("tokens")
+        need("tokens", "first", "mix", "second", "gain", "bias", "spatial_w", "spatial_b")
         exchange_tokens.wait()
 
         def body(r):
@@ -338,10 +353,13 @@
                 [wide[20 + j, nb // 2, pl.ds(2 * (nb % 2), 2)].reshape(512, 256) for j in range(2)],
                 axis=1)
             part[r, 512 * nb : 512 * nb + 512] = dot_t(mixed[r], right).astype(BF)
-        exchange_mix[h].start()
+            if nb:
+                exchange_mix[h][nb - 1].start()
+        exchange_mix[h][3].start()
 
     def combine_mix(h):
-        exchange_mix[h].wait()
+        for block in exchange_mix[h]:
+            block.wait()
 
         def body(r):
             branch = part[r].astype(F32) + got_mix[r].astype(F32)
@@ -365,13 +383,16 @@
         for nb in range(2):
             c = slice(512 * nb, 512 * nb + 512)
             last_part[r, c] = down_rows(h, 1 - tp, 2 * nb).astype(BF)
-        exchange_last[h].start()
+            if nb:
+                exchange_last[h][0].start()
+        exchange_last[h][1].start()
         for nb in range(2):
             c = slice(512 * nb, 512 * nb + 512)
             part[r, c] = down_rows(h, tp, 2 * nb).astype(BF)
 
     def finish(h):
-        exchange_last[h].wait()
+        for block in exchange_last[h]:
+            block.wait()
 
         def body(r):
             own = middle[r, pl.ds(pl.multiple_of(tp * 1024, 1024), 1024)].astype(F32)
@@ -419,12 +440,16 @@
     return pl.pallas_call(
         kernel,
         out_shape=jax.ShapeDtypeStruct(tokens.shape, BF),
-        in_specs=[
-            pl.BlockSpec(memory_space=pl.ANY if n in (0, 4, 5, 6, 10, 11, 18) else pltpu.VMEM)
-            for n in range(20)
-        ],
+        in_specs=[pl.BlockSpec(memory_space=pl.ANY)] * 20,
         out_specs=pl.BlockSpec(memory_space=pl.ANY),
         scratch_shapes=[
+            *[vmem((1, 2048), F32)] * 3,
+            *[vmem((11, 128), F32)] * 2,
+            vmem((1, 64), F32),
+            *[vmem((1, 512), F32)] * 4,
+            vmem((4, 128, 128), BF),
+            vmem((4, 128), F32),
+            vmem((1, 64), F32),
             *[vmem((64, 1408), F32)] * 3,
             *[vmem((64, 512), F32)] * 3,
             vmem((N_UNITS - 1, 2, 4, 4, 64, 256), BF),
@@ -445,7 +470,7 @@
             vmem((rows, 128), F32),
             pltpu.SemaphoreType.DMA((N_UNITS, 5)),
             pltpu.SemaphoreType.DMA((N_UNITS, 5)),
-            *[pltpu.SemaphoreType.DMA((n,)) for n in (9, 9, 7, 2)],
+            *[pltpu.SemaphoreType.DMA((n,)) for n in (17, 17, 20, 2)],
         ],
         compiler_params=pltpu.CompilerParams(
             collective_id=0, has_side_effects=True, vmem_limit_bytes=67043328

time: 126 us -> 124 us (0.984)
  no operation moved by 1% of the time
where the time goes in v3:
time: 124 us
  Pallas kernels  122 us (98%)
  local copies, waits for them, and re-layouts  2.47 us (2%)
    pallas_call x1, Pallas kernels, on_device(): pl.pallas_call(kernel, out_shape=jax.ShapeDtypeStruct(tokens.shape, BF),...  122 us

profile of v3, /device:TPU:1, one launch (start us, length us, event | category | flops | bytes accessed | tf_op | source)
XLA Modules:
  0.0 124.3 jit_solution(13847319116843839793)
XLA Ops:
  0.0 121.8 %shard_map.190 = bf16[640,1024]{1,0:T(8,128)(2,1)} custom-call(bf16[640,1024]{1,0:T(8,128)(2,1)} %tokens.1, f32[1,2048]{1,0:T(1,128)} %bitcast.15, f32[1,2048]{1,0:T(1,128)} %bitcast.16, f32[1,2048]{1,0:T(1,128)} %bitcast.17, f32[64,1408]{1,0:T(8,128)} %gate_hbm.1, f32[64,1408]{1,0:T(8,128)} %up_hbm.1, f32[64,1408]{1,0:T(8,128)} %bitcast.13, ...), custom_call_target="tpu_custom_call" | custom-call | tf_op jit(solution)/shard_map/pallas_call | solution.py:440
  121.8 2.5 %copy.22 = bf16[640,1024]{1,0:T(8,128)(2,1)} copy(bf16[640,1024]{1,0:T(8,128)(2,1)} %shard_map.190) | data formatting | bytes 2621440

commit v4 on v3

--- a/solution.py
+++ b/solution.py
@@ -34,7 +34,7 @@
     1140, 1141, 205, 195, 1150, 1151, 1160, 215, 1161, 225, 1170, 1171,
 )
 
-GROUPS_OF_ROWS = ((0, 384), (384, 256))
+GROUPS_OF_ROWS = ((0, 256), (256, 384))
 STEP_ROWS = 16
 UNROLL = 8
 PLACED_AHEAD = 4

time: 124 us -> 126 us (1.016)
  no operation moved by 1% of the time
where the time goes in v4:
time: 126 us; the launch traced here: 125 us
  Pallas kernels  123 us (98%)
  local copies, waits for them, and re-layouts  2.47 us (2%)
    pallas_call x1, Pallas kernels, on_device(): pl.pallas_call(kernel, out_shape=jax.ShapeDtypeStruct(tokens.shape, BF),...  123 us

profile of v4, /device:TPU:1, one launch (start us, length us, event | category | flops | bytes accessed | tf_op | source)
XLA Modules:
  0.0 125.4 jit_solution(10270491604720371262)
XLA Ops:
  0.0 122.9 %shard_map.190 = bf16[640,1024]{1,0:T(8,128)(2,1)} custom-call(bf16[640,1024]{1,0:T(8,128)(2,1)} %tokens.1, f32[1,2048]{1,0:T(1,128)} %bitcast.15, f32[1,2048]{1,0:T(1,128)} %bitcast.16, f32[1,2048]{1,0:T(1,128)} %bitcast.17, f32[64,1408]{1,0:T(8,128)} %gate_hbm.1, f32[64,1408]{1,0:T(8,128)} %up_hbm.1, f32[64,1408]{1,0:T(8,128)} %bitcast.13, ...), custom_call_target="tpu_custom_call" | custom-call | tf_op jit(solution)/shard_map/pallas_call | solution.py:440
  122.9 2.5 %copy.22 = bf16[640,1024]{1,0:T(8,128)(2,1)} copy(bf16[640,1024]{1,0:T(8,128)(2,1)} %shard_map.190) | data formatting | bytes 2621440
